TPU v7x, 32 devices: a whole 2x2x4 slice. The times are simulated.
32 devices in a mesh: rep: 4 (over z), fs: 4 (over y, x), tp: 2 (over core).
Axes of the slice: x: 2, y: 2, z: 4, core: 2. Of those that a mesh axis runs over, the one named last changes fastest.
Arguments:
- tokens: bfloat16 [8192, 2048], P(('rep', 'fs')), may hold values from -6 to 6
- mix_gain: float32 [2048], replicated, may hold values from 0.1 to 1.9
- w_gate_b: bfloat16 [2048, 1024], P('fs', 'tp'), may hold values from -0.125 to 0.125
- w_gate_c: bfloat16 [2048, 1024], P('fs', 'tp'), may hold values from -0.125 to 0.125
- w_conv_in: bfloat16 [2048, 1024], P('fs', 'tp'), may hold values from -0.125 to 0.125
- conv_taps: float32 [3, 1024], P(None, 'tp'), may hold values from -3 to 3
- w_mix_out: bfloat16 [1024, 2048], P('tp', 'fs'), may hold values from -0.1875 to 0.1875
- ffn_gain: float32 [2048], replicated, may hold values from 0.1 to 1.9
- w_ffn_gate: bfloat16 [2048, 2816], P('fs', 'tp'), may hold values from -0.125 to 0.125
- w_ffn_up: bfloat16 [2048, 2816], P('fs', 'tp'), may hold values from -0.125 to 0.125
- w_ffn_down: bfloat16 [2816, 2048], P('tp', 'fs'), may hold values from -0.109375 to 0.109375
Outputs:
- layer_out: bfloat16 [8192, 2048], P(('rep', 'fs', 'tp'))
All inputs are finite; a program needn't handle non-finite values.
Results may differ from a plain program's by a relative error of at most 0.014.
Values may be sent and summed in bfloat16 or wider, within the bound.
A program may use at most 64 MiB of HBM per device.

v0:
```python
import jax
import jax.numpy as jnp
from jax import lax
from jax.sharding import PartitionSpec as P

LEN = 128
EPSILON = 1e-06


def rms_scale(values, gain):
    return values * lax.rsqrt(jnp.mean(values * values, axis=-1, keepdims=True) + EPSILON) * gain


def causal_mix(product_in, conv_taps):
    shaped = product_in.reshape(product_in.shape[0] // LEN, LEN, product_in.shape[1])
    padded = jnp.pad(shaped, ((0, 0), (2, 0), (0, 0)))
    convolved = (
        conv_taps[0] * padded[:, :-2]
        + conv_taps[1] * padded[:, 1:-1]
        + conv_taps[2] * padded[:, 2:]
    )
    return convolved.reshape(product_in.shape)


def local(
    tokens,
    mix_gain,
    w_gate_b,
    w_gate_c,
    w_conv_in,
    conv_taps,
    w_mix_out,
    ffn_gain,
    w_ffn_gate,
    w_ffn_up,
    w_ffn_down,
):
    normed = rms_scale(tokens.astype(jnp.float32), mix_gain).astype(jnp.bfloat16)
    shard_rows = (
        lax.all_gather(w_gate_b, "fs", axis=0, tiled=True),
        lax.all_gather(w_gate_c, "fs", axis=0, tiled=True),
        lax.all_gather(w_conv_in, "fs", axis=0, tiled=True),
    )
    gate_b, gate_c, conv_in = tuple(
        (jnp.dot(normed, weight, preferred_element_type=jnp.float32) for weight in shard_rows)
    )
    gated = (gate_b * causal_mix(gate_c * conv_in, conv_taps)).astype(jnp.bfloat16)
    mix_columns = lax.all_gather(w_mix_out, "fs", axis=1, tiled=True)
    row_count = normed.shape[0] // lax.axis_size("tp")
    branch = lax.psum_scatter(
        jnp.dot(gated, mix_columns, preferred_element_type=jnp.float32).astype(jnp.bfloat16),
        "tp",
        scatter_dimension=0,
        tiled=True,
    ).astype(jnp.float32)
    own_rows = lax.dynamic_slice_in_dim(tokens, lax.axis_index("tp") * row_count, row_count, 0)
    stream = own_rows.astype(jnp.float32) + branch
    normed_two = rms_scale(stream, ffn_gain).astype(jnp.bfloat16)
    gate_rows, up_rows = (
        lax.all_gather(w_ffn_gate, "fs", axis=0, tiled=True),
        lax.all_gather(w_ffn_up, "fs", axis=0, tiled=True),
    )
    shard_rows = lax.all_gather(normed_two, "tp", axis=0, tiled=True)
    gate_part = jnp.dot(shard_rows, gate_rows, preferred_element_type=jnp.float32)
    up_part = jnp.dot(shard_rows, up_rows, preferred_element_type=jnp.float32)
    hidden = (jax.nn.silu(gate_part) * up_part).astype(jnp.bfloat16)
    down_columns = lax.all_gather(w_ffn_down, "fs", axis=1, tiled=True)
    ffn_branch = lax.psum_scatter(
        jnp.dot(hidden, down_columns, preferred_element_type=jnp.float32).astype(jnp.bfloat16),
        "tp",
        scatter_dimension=0,
        tiled=True,
    ).astype(jnp.float32)
    return (stream + ffn_branch).astype(jnp.bfloat16)


def solution(mesh):
    in_specs = (
        P(("rep", "fs"), None),
        P(),
        P("fs", "tp"),
        P("fs", "tp"),
        P("fs", "tp"),
        P(None, "tp"),
        P("tp", "fs"),
        P(),
        P("fs", "tp"),
        P("fs", "tp"),
        P("tp", "fs"),
    )
    out_specs = P(("rep", "fs", "tp"), None)
    return jax.shard_map(local, mesh=mesh, in_specs=in_specs, out_specs=out_specs, check_vma=False)
```

profile of v0, /device:TPU:0, one launch (start us, length us, event | category | flops | bytes accessed | tf_op | source)
XLA Modules:
  0.0 424.1 jit_solution(1093069393383213584)
XLA Ops:
  6.5 0.0 copy-start
  6.5 0.0 all-gather.11.cloned.1.call-start
  6.5 0.0 copy-start.3
  6.5 0.0 copy-start.4
  6.5 0.7 all-gather.11.cloned.1.call-update
  7.3 0.0 all-gather.13.cloned.1.call-start
  7.3 0.7 all-gather.13.cloned.1.call-update
  8.0 0.0 all-gather.15.cloned.1.call-start
  8.1 0.7 all-gather.15.cloned.1.call-update
  8.7 0.0 all-gather.9.cloned.1.call-start
  8.8 0.5 all-gather.9.cloned.1.call-update
  9.3 0.0 reduce-scatter.3.cloned.1.call-start
  9.4 0.0 copy-done
  9.4 0.5 fusion
  9.9 0.0 copy-done.3
  9.9 37.2 %all-gather.11.cloned.1.call-done = bf16[2048,512]{1,0:T(8,128)(2,1)} async-done(((bf16[512,512]{1,0:T(8,128)(2,1)}), bf16[2048,512]{1,0:T(8,128)(2,1)}) %all-gather.11.cloned.1.call-update) | async-done | bytes 2097168 | tf_op jit(solution)/shard_map/all_gather | solution.py:41
  47.1 0.0 copy-done.4
  47.1 2.9 fusion.11
  50.0 34.2 %all-gather.13.cloned.1.call-done = bf16[2048,512]{1,0:T(8,128)(2,1)} async-done(((bf16[512,512]{1,0:T(8,128)(2,1)}), bf16[2048,512]{1,0:T(8,128)(2,1)}) %all-gather.13.cloned.1.call-update) | async-done | bytes 2097168 | tf_op jit(solution)/shard_map/all_gather | solution.py:42
  84.2 2.9 convolution_multiply_fusion.1
  87.1 0.3 fusion.7
  87.4 33.7 %all-gather.15.cloned.1.call-done = bf16[512,2048]{1,0:T(8,128)(2,1)} async-done(((bf16[512,512]{1,0:T(8,128)(2,1)}), bf16[512,2048]{1,0:T(8,128)(2,1)}) %all-gather.15.cloned.1.call-update) | async-done | bytes 2097168 | tf_op jit(solution)/shard_map/all_gather | solution.py:48
  121.1 36.9 %all-gather.9.cloned.1.call-done = bf16[2048,512]{1,0:T(8,128)(2,1)} async-done(((bf16[512,512]{1,0:T(8,128)(2,1)}), bf16[2048,512]{1,0:T(8,128)(2,1)}) %all-gather.9.cloned.1.call-update) | async-done | bytes 2097168 | tf_op jit(solution)/shard_map/all_gather | solution.py:40
  158.0 5.9 %convolution_convert_fusion = bf16[512,2048]{1,0:T(8,128)(2,1)} fusion(bf16[512,2048]{1,0:T(8,128)(2,1)} %all-gather.15.cloned.1.call-done, f32[512,512]{1,0:T(8,128)S(1)} %bitcast.14, bf16[2048,512]{1,0:T(8,128)(2,1)} %all-gather.9.cloned.1.call-done, bf16[512,2048]{1,0:T(8,128)(2,1)S(1)} %copy-done, f32[2048]{0:T(1024)S(1)} %copy-done.4, ...), kind=kOutput, calls=%fused_computation.7 | convolution fusion | flops 2153250816 | bytes 9447424 | tf_op jit(solution)/shard_map/dot_general | solution.py:51
  163.9 0.0 reduce-scatter.3.cloned.1.call-update
  163.9 0.0 copy-start.2
  164.0 0.0 all-gather.19.cloned.1.call-start
  164.0 0.5 all-gather.19.cloned.1.call-update
  164.5 0.0 all-gather.17.cloned.1.call-start
  164.6 9.3 %reduce-scatter.3.cloned.1.call-done = bf16[256,2048]{1,0:T(8,128)(2,1)} async-done(((bf16[512,2048]{1,0:T(8,128)(2,1)}), bf16[256,2048]{1,0:T(8,128)(2,1)}) %reduce-scatter.3.cloned.1.call-update) | async-done | bytes 1048592 | tf_op jit(solution)/shard_map/reduce_scatter | solution.py:50
  173.9 0.0 copy-start.1
  173.9 1.7 multiply_reduce_fusion
  175.6 0.0 copy-done.2
  175.6 0.0 copy-done.1
  175.6 1.5 multiply_convert_fusion
  177.1 0.0 all-gather.17.cloned.1.call-update
  177.1 0.0 all-gather.21.cloned.1.call-start
  177.2 0.7 all-gather.21.cloned.1.call-update
  177.9 0.0 all-gather.23.cloned.1.call-start
  177.9 0.7 all-gather.23.cloned.1.call-update
  178.6 0.2 reduce-scatter.5.cloned.1.call-start
  178.8 63.7 %all-gather.19.cloned.1.call-done = bf16[2048,1408]{1,0:T(8,128)(2,1)} async-done(((bf16[512,1408]{1,0:T(8,128)(2,1)}), bf16[2048,1408]{1,0:T(8,128)(2,1)}) %all-gather.19.cloned.1.call-update) | async-done | bytes 5767184 | tf_op jit(solution)/shard_map/all_gather | solution.py:60
  242.5 12.1 %all-gather.17.cloned.1.call-done = bf16[512,2048]{1,0:T(8,128)(2,1)} async-done(((bf16[256,2048]{1,0:T(8,128)(2,1)}), bf16[512,2048]{1,0:T(8,128)(2,1)}) %all-gather.17.cloned.1.call-update) | async-done | bytes 2097168 | tf_op jit(solution)/shard_map/all_gather | solution.py:63
  254.7 8.2 %fusion.16 = f32[512,1408]{1,0:T(8,128)} fusion(bf16[512,2048]{1,0:T(8,128)(2,1)} %all-gather.17.cloned.1.call-done, bf16[2048,1408]{1,0:T(8,128)(2,1)} %all-gather.19.cloned.1.call-done), kind=kOutput, calls=%fused_computation.27 | convolution fusion | flops 2952790016 | bytes 10747904 | tf_op jit(solution)/shard_map/dot_general | solution.py:64
  262.9 60.5 %all-gather.21.cloned.1.call-done = bf16[2048,1408]{1,0:T(8,128)(2,1)} async-done(((bf16[512,1408]{1,0:T(8,128)(2,1)}), bf16[2048,1408]{1,0:T(8,128)(2,1)}) %all-gather.21.cloned.1.call-update) | async-done | bytes 5767184 | tf_op jit(solution)/shard_map/all_gather | solution.py:61
  323.4 67.4 %all-gather.23.cloned.1.call-done = bf16[1408,2048]{1,0:T(8,128)(2,1)} async-done(((bf16[1408,512]{1,0:T(8,128)(2,1)}), bf16[1408,2048]{1,0:T(8,128)(2,1)}) %all-gather.23.cloned.1.call-update) | async-done | bytes 5767184 | tf_op jit(solution)/shard_map/all_gather | solution.py:67
  390.8 13.8 %convolution_convert_fusion.1 = bf16[512,2048]{1,0:T(8,128)(2,1)} fusion(bf16[1408,2048]{1,0:T(8,128)(2,1)} %all-gather.23.cloned.1.call-done, bf16[512,2048]{1,0:T(8,128)(2,1)} %all-gather.17.cloned.1.call-done, bf16[2048,1408]{1,0:T(8,128)(2,1)} %all-gather.21.cloned.1.call-done, f32[512,1408]{1,0:T(8,128)} %fusion.16), kind=kOutput, calls=%fused_computation.8 | convolution fusion | flops 5910953984 | bytes 18612224 | tf_op jit(solution)/shard_map/dot_general | solution.py:69
  404.6 0.0 reduce-scatter.5.cloned.1.call-update
  404.6 9.9 %reduce-scatter.5.cloned.1.call-done = bf16[256,2048]{1,0:T(8,128)(2,1)} async-done(((bf16[512,2048]{1,0:T(8,128)(2,1)}), bf16[256,2048]{1,0:T(8,128)(2,1)}) %reduce-scatter.5.cloned.1.call-update) | async-done | bytes 1048592 | tf_op jit(solution)/shard_map/reduce_scatter | solution.py:68
  414.5 2.7 add_convert_fusion
  (3 shorter events, 0.0 us)
Async XLA Ops:
  6.5 2.8 copy-start
  6.5 40.6 %all-gather.11.cloned.1.call-start = ((), (), s32[]{:S(2)}) async-start(), calls=%async_computation.3 | async-start | bytes 2621440 | tf_op jit(solution)/shard_map/all_gather | solution.py:41
  6.5 3.3 copy-start.3
  6.5 40.6 %copy-start.4 = (f32[2048]{0:T(1024)S(1)}, f32[2048]{0:T(1024)}, u32[]{:S(2)}) copy-start(f32[2048]{0:T(1024)} %param.12) | copy-start | bytes 24580
  7.3 76.9 %all-gather.13.cloned.1.call-start = ((), (), s32[]{:S(2)}) async-start(), calls=%async_computation.4 | async-start | bytes 2621440 | tf_op jit(solution)/shard_map/all_gather | solution.py:42
  8.0 113.1 %all-gather.15.cloned.1.call-start = ((), (), s32[]{:S(2)}) async-start(), calls=%async_computation.5 | async-start | bytes 2621440 | tf_op jit(solution)/shard_map/all_gather | solution.py:48
  8.7 149.2 %all-gather.9.cloned.1.call-start = ((), (), s32[]{:S(2)}) async-start(), calls=%async_computation.2 | async-start | bytes 2621440 | tf_op jit(solution)/shard_map/all_gather | solution.py:40
  9.3 164.5 %reduce-scatter.3.cloned.1.call-start = ((), (), s32[]{:S(2)}) async-start(), calls=%async_computation.6 | async-start | bytes 3145728 | tf_op jit(solution)/shard_map/reduce_scatter | solution.py:50
  163.9 11.7 %copy-start.2 = (f32[2048]{0:T(1024)S(1)}, f32[2048]{0:T(1024)}, u32[]{:S(2)}) copy-start(f32[2048]{0:T(1024)} %param.18) | copy-start | bytes 24580
  164.0 78.6 %all-gather.19.cloned.1.call-start = ((), (), s32[]{:S(2)}) async-start(), calls=%async_computation.8 | async-start | bytes 7208960 | tf_op jit(solution)/shard_map/all_gather | solution.py:60
  164.5 90.2 %all-gather.17.cloned.1.call-start = ((), (), s32[]{:S(2)}) async-start(), calls=%async_computation.7 | async-start | bytes 3145728 | tf_op jit(solution)/shard_map/all_gather | solution.py:63
  173.9 1.8 copy-start.1
  177.1 146.3 %all-gather.21.cloned.1.call-start = ((), (), s32[]{:S(2)}) async-start(), calls=%async_computation.9 | async-start | bytes 7208960 | tf_op jit(solution)/shard_map/all_gather | solution.py:61
  177.9 212.9 %all-gather.23.cloned.1.call-start = ((), (), s32[]{:S(2)}) async-start(), calls=%async_computation.10 | async-start | bytes 7208960 | tf_op jit(solution)/shard_map/all_gather | solution.py:67
  178.6 235.9 %reduce-scatter.5.cloned.1.call-start = ((), (), s32[]{:S(2)}) async-start(), calls=%async_computation.11 | async-start | bytes 3145728 | tf_op jit(solution)/shard_map/reduce_scatter | solution.py:68
Sparse Core Ops, SparseCore 0:
  9.2 37.8 all-gather.10
  49.0 35.1 all-gather.12
  86.0 35.0 all-gather.14
  122.8 35.1 all-gather.8
  164.1 9.7 reduce-scatter.2
  175.6 66.9 all-gather.18
  244.1 10.5 all-gather.16
  256.5 66.8 all-gather.20
  325.2 65.5 all-gather.22
  404.8 9.7 reduce-scatter.4
where the time goes:
time: 424 us
  waiting for transfers between devices  369 us (87%)
  matrix products  33.8 us (8%)
  between operations  13.6 us (3%)
  other arithmetic  6.75 us (2%)
    all_gather x1, waiting for transfers between devices, local(): down_columns = lax.all_gather(w_ffn_down, 'fs', axis=1, tiled=True)  67.4 us
    all_gather x1, waiting for transfers between devices, local(): lax.all_gather(w_ffn_gate, 'fs', axis=0, tiled=True)  63.7 us
    all_gather x1, waiting for transfers between devices, local(): lax.all_gather(w_ffn_up, 'fs', axis=0, tiled=True)  60.5 us
    all_gather x1, waiting for transfers between devices, local(): lax.all_gather(w_gate_c, 'fs', axis=0, tiled=True)  37.2 us
    all_gather x1, waiting for transfers between devices, local(): lax.all_gather(w_gate_b, 'fs', axis=0, tiled=True)  36.9 us
    all_gather x1, waiting for transfers between devices, local(): lax.all_gather(w_conv_in, 'fs', axis=0, tiled=True)  34.2 us
    all_gather x1, waiting for transfers between devices, local(): mix_columns = lax.all_gather(w_mix_out, 'fs', axis=1, tiled=True)  33.7 us
    dot_general x1, matrix products, local(): jnp.dot(hidden, down_columns, preferred_element_type=jnp.float32)  13.8 us
  transfers between devices with their start and end apart: 10, of which 10 were waited for; matrix products, arithmetic and copies ran while one was open for 4% of the time, Pallas kernels for 0%

commit v1 on v0

--- a/solution.py
+++ b/solution.py
@@ -45,7 +45,12 @@
         (jnp.dot(normed, weight, preferred_element_type=jnp.float32) for weight in shard_rows)
     )
     gated = (gate_b * causal_mix(gate_c * conv_in, conv_taps)).astype(jnp.bfloat16)
-    mix_columns = lax.all_gather(w_mix_out, "fs", axis=1, tiled=True)
+    ring = [w_mix_out]
+    for hop in range(3):
+        ring.append(lax.ppermute(ring[-1], "fs", [(dev, (dev + 1) % 4) for dev in range(4)]))
+    mix_columns = jnp.roll(
+        jnp.concatenate(ring[::-1], axis=1), (lax.axis_index("fs") + 1) * ring[0].shape[1], axis=1
+    )
     row_count = normed.shape[0] // lax.axis_size("tp")
     branch = lax.psum_scatter(
         jnp.dot(gated, mix_columns, preferred_element_type=jnp.float32).astype(jnp.bfloat16),

time: 424 us -> 400 us (0.943)
  waiting for transfers between devices: 369 us -> 325 us
  local copies, waits for them, and re-layouts: 0.03 us -> 9.27 us
  starting transfers between devices: 0.53 us -> 8.37 us
    ppermute x0 -> x3, waiting for transfers between devices: none -> 45.4 us  [local(): lax.ppermute(ring[-1], 'fs', [(dev, (dev + 1) % 4) for dev in range(4)])]
    all_gather x1, waiting for transfers between devices: 37.2 us -> 0.01 us  [local(): lax.all_gather(w_gate_c, 'fs', axis=0, tiled=True)]
    all_gather x1 -> x0, waiting for transfers between devices: 33.7 us -> none  [local(): mix_columns = lax.all_gather(w_mix_out, 'fs', axis=1, tiled=True)]
    all_gather x1, waiting for transfers between devices: 34.2 us -> 21.2 us  [local(): lax.all_gather(w_conv_in, 'fs', axis=0, tiled=True)]
    unnamed x10 -> x23, local copies, waits for them, and re-layouts: 0.02 us -> 8.41 us
    ppermute x0 -> x3, starting transfers between devices: none -> 7.88 us  [local(): lax.ppermute(ring[-1], 'fs', [(dev, (dev + 1) % 4) for dev in range(4)])]
  transfers between devices with their start and end apart: 10 -> 12, of which waited for: 10 -> 11; matrix products, arithmetic and copies ran while one was open for 4% -> 7% of each run, Pallas kernels for 0% -> 0%
where the time goes in v1:
time: 400 us
  waiting for transfers between devices  325 us (81%)
  matrix products  33.8 us (8%)
  between operations  13.3 us (3%)
  other arithmetic  9.35 us (2%)
  local copies, waits for them, and re-layouts  9.27 us (2%)
  starting transfers between devices  8.37 us (2%)
    all_gather x1, waiting for transfers between devices, local(): down_columns = lax.all_gather(w_ffn_down, 'fs', axis=1, tiled=True)  67.4 us
    all_gather x1, waiting for transfers between devices, local(): lax.all_gather(w_ffn_gate, 'fs', axis=0, tiled=True)  62.7 us
    all_gather x1, waiting for transfers between devices, local(): lax.all_gather(w_ffn_up, 'fs', axis=0, tiled=True)  60.5 us
    ppermute x3, waiting for transfers between devices, local(): lax.ppermute(ring[-1], 'fs', [(dev, (dev + 1) % 4) for dev in range(4)])  45.4 us
    all_gather x1, waiting for transfers between devices, local(): lax.all_gather(w_gate_b, 'fs', axis=0, tiled=True)  33.8 us
    all_gather x1, waiting for transfers between devices, local(): lax.all_gather(w_conv_in, 'fs', axis=0, tiled=True)  21.2 us
    dot_general x1, matrix products, local(): jnp.dot(hidden, down_columns, preferred_element_type=jnp.float32)  13.8 us
    all_gather x1, waiting for transfers between devices, local(): shard_rows = lax.all_gather(normed_two, 'tp', axis=0, tiled=True)  12 us
  transfers between devices with their start and end apart: 12, of which 11 were waited for; matrix products, arithmetic and copies ran while one was open for 7% of the time, Pallas kernels for 0%

profile of v1, /device:TPU:0, one launch (start us, length us, event | category | flops | bytes accessed | tf_op | source)
XLA Modules:
  0.0 399.6 jit_solution(15482642217624675825)
XLA Ops:
  6.5 0.0 copy-start.6
  6.5 0.0 all-gather.10.cloned.1.call-start
  6.5 0.7 all-gather.10.cloned.1.call-update
  7.3 0.0 all-gather.12.cloned.1.call-start
  7.3 0.7 all-gather.12.cloned.1.call-update
  8.0 0.0 copy-start.2
  8.0 0.0 all-gather.8.cloned.1.call-start
  8.1 3.0 collective-permute-start
  11.1 15.3 %collective-permute-done = bf16[512,512]{1,0:T(8,128)(2,1)S(1)} collective-permute-done((bf16[512,512]{1,0:T(8,128)(2,1)}, bf16[512,512]{1,0:T(8,128)(2,1)S(1)}, u32[]{:S(2)}, u32[]{:S(2)}) %collective-permute-start) | collective-permute-done | bytes 524320 | tf_op jit(solution)/shard_map/ppermute | solution.py:50
  26.4 2.4 collective-permute-start.1
  28.8 0.0 all-gather.8.cloned.1.call-update
  28.8 0.0 reduce-scatter.3.cloned.1.call-start
  28.9 15.4 %collective-permute-done.1 = bf16[512,512]{1,0:T(8,128)(2,1)S(1)} collective-permute-done((bf16[512,512]{1,0:T(8,128)(2,1)S(1)}, bf16[512,512]{1,0:T(8,128)(2,1)S(1)}, u32[]{:S(2)}, u32[]{:S(2)}) %collective-permute-start.1) | collective-permute-done | bytes 524320 | tf_op jit(solution)/shard_map/ppermute | solution.py:50
  44.3 0.0 copy-start.3
  44.3 2.5 collective-permute-start.2
  46.8 2.1 fusion
  48.9 0.0 copy-done.6
  48.9 14.6 %collective-permute-done.2 = bf16[512,512]{1,0:T(8,128)(2,1)S(1)} collective-permute-done((bf16[512,512]{1,0:T(8,128)(2,1)S(1)}, bf16[512,512]{1,0:T(8,128)(2,1)S(1)}, u32[]{:S(2)}, u32[]{:S(2)}) %collective-permute-start.2) | collective-permute-done | bytes 524320 | tf_op jit(solution)/shard_map/ppermute | solution.py:50
  63.5 0.9 constant_dynamic-update-slice_fusion.7
  64.4 0.9 constant_dynamic-update-slice_fusion.6
  65.3 0.0 copy-done.3
  65.3 0.0 copy-done.4
  65.3 0.9 constant_dynamic-update-slice_fusion.5
  66.2 0.0 copy-done.2
  66.2 0.0 copy-start
  66.2 0.0 copy-start.7
  66.2 0.9 constant_dynamic-update-slice_fusion.4
  67.2 2.0 constant_dynamic-update-slice_fusion.3
  69.1 1.9 constant_dynamic-update-slice_fusion.2
  71.0 0.9 constant_dynamic-update-slice_fusion.1
  71.9 0.8 constant_dynamic-update-slice_fusion
  72.7 0.0 all-gather.10.cloned.1.call-done
  72.7 0.0 copy-done
  72.8 0.0 copy-done.7
  72.8 2.9 fusion.13
  75.6 21.2 %all-gather.12.cloned.1.call-done = bf16[2048,512]{1,0:T(8,128)(2,1)} async-done(((bf16[512,512]{1,0:T(8,128)(2,1)}), bf16[2048,512]{1,0:T(8,128)(2,1)}) %all-gather.12.cloned.1.call-update) | async-done | bytes 2097168 | tf_op jit(solution)/shard_map/all_gather | solution.py:42
  96.8 2.9 convolution_multiply_fusion.1
  99.7 0.3 fusion.8
  100.0 33.8 %all-gather.8.cloned.1.call-done = bf16[2048,512]{1,0:T(8,128)(2,1)} async-done(((bf16[512,512]{1,0:T(8,128)(2,1)}), bf16[2048,512]{1,0:T(8,128)(2,1)}) %all-gather.8.cloned.1.call-update) | async-done | bytes 2097168 | tf_op jit(solution)/shard_map/all_gather | solution.py:40
  133.9 6.0 %convolution_convert_fusion = bf16[512,2048]{1,0:T(8,128)(2,1)} fusion(bf16[512,4096]{1,0:T(8,128)(2,1)} %constant_dynamic-update-slice_fusion, s32[]{:T(128)S(6)} %select_n.18, f32[512,512]{1,0:T(8,128)S(1)} %bitcast.13, bf16[2048,512]{1,0:T(8,128)(2,1)} %all-gather.8.cloned.1.call-done, bf16[512,2048]{1,0:T(8,128)(2,1)S(1)} %copy-done, ...), kind=kOutput, calls=%fused_computation.7 | convolution fusion | flops 2153250816 | bytes 9447428 | tf_op jit(solution)/shard_map/dot_general | solution.py:56
  139.9 0.0 reduce-scatter.3.cloned.1.call-update
  139.9 0.0 all-gather.16.cloned.1.call-start
  140.0 0.5 all-gather.16.cloned.1.call-update
  140.5 0.0 all-gather.14.cloned.1.call-start
  140.6 9.3 %reduce-scatter.3.cloned.1.call-done = bf16[256,2048]{1,0:T(8,128)(2,1)} async-done(((bf16[512,2048]{1,0:T(8,128)(2,1)}), bf16[256,2048]{1,0:T(8,128)(2,1)}) %reduce-scatter.3.cloned.1.call-update) | async-done | bytes 1048592 | tf_op jit(solution)/shard_map/reduce_scatter | solution.py:55
  149.8 1.6 multiply_reduce_fusion
  151.5 0.0 copy-done.5
  151.5 2.6 multiply_convert_fusion
  154.1 0.0 all-gather.14.cloned.1.call-update
  154.1 0.0 all-gather.18.cloned.1.call-start
  154.2 0.7 all-gather.18.cloned.1.call-update
  154.9 0.0 all-gather.20.cloned.1.call-start
  154.9 0.7 all-gather.20.cloned.1.call-update
  155.6 0.2 reduce-scatter.5.cloned.1.call-start
  155.8 62.7 %all-gather.16.cloned.1.call-done = bf16[2048,1408]{1,0:T(8,128)(2,1)} async-done(((bf16[512,1408]{1,0:T(8,128)(2,1)}), bf16[2048,1408]{1,0:T(8,128)(2,1)}) %all-gather.16.cloned.1.call-update) | async-done | bytes 5767184 | tf_op jit(solution)/shard_map/all_gather | solution.py:65
  218.5 12.0 %all-gather.14.cloned.1.call-done = bf16[512,2048]{1,0:T(8,128)(2,1)} async-done(((bf16[256,2048]{1,0:T(8,128)(2,1)}), bf16[512,2048]{1,0:T(8,128)(2,1)}) %all-gather.14.cloned.1.call-update) | async-done | bytes 2097168 | tf_op jit(solution)/shard_map/all_gather | solution.py:68
  230.5 8.3 %fusion.18 = f32[512,1408]{1,0:T(8,128)} fusion(bf16[512,2048]{1,0:T(8,128)(2,1)} %all-gather.14.cloned.1.call-done, bf16[2048,1408]{1,0:T(8,128)(2,1)} %all-gather.16.cloned.1.call-done), kind=kOutput, calls=%fused_computation.37 | convolution fusion | flops 2952790016 | bytes 10747904 | tf_op jit(solution)/shard_map/dot_general | solution.py:69
  238.8 60.5 %all-gather.18.cloned.1.call-done = bf16[2048,1408]{1,0:T(8,128)(2,1)} async-done(((bf16[512,1408]{1,0:T(8,128)(2,1)}), bf16[2048,1408]{1,0:T(8,128)(2,1)}) %all-gather.18.cloned.1.call-update) | async-done | bytes 5767184 | tf_op jit(solution)/shard_map/all_gather | solution.py:66
  299.2 67.4 %all-gather.20.cloned.1.call-done = bf16[1408,2048]{1,0:T(8,128)(2,1)} async-done(((bf16[1408,512]{1,0:T(8,128)(2,1)}), bf16[1408,2048]{1,0:T(8,128)(2,1)}) %all-gather.20.cloned.1.call-update) | async-done | bytes 5767184 | tf_op jit(solution)/shard_map/all_gather | solution.py:72
  366.6 13.8 %convolution_convert_fusion.1 = bf16[512,2048]{1,0:T(8,128)(2,1)} fusion(bf16[1408,2048]{1,0:T(8,128)(2,1)} %all-gather.20.cloned.1.call-done, bf16[512,2048]{1,0:T(8,128)(2,1)} %all-gather.14.cloned.1.call-done, bf16[2048,1408]{1,0:T(8,128)(2,1)} %all-gather.18.cloned.1.call-done, f32[512,1408]{1,0:T(8,128)} %fusion.18), kind=kOutput, calls=%fused_computation.8 | convolution fusion | flops 5910953984 | bytes 18612224 | tf_op jit(solution)/shard_map/dot_general | solution.py:74
  380.4 0.0 reduce-scatter.5.cloned.1.call-update
  380.5 9.9 %reduce-scatter.5.cloned.1.call-done = bf16[256,2048]{1,0:T(8,128)(2,1)} async-done(((bf16[512,2048]{1,0:T(8,128)(2,1)}), bf16[256,2048]{1,0:T(8,128)(2,1)}) %reduce-scatter.5.cloned.1.call-update) | async-done | bytes 1048592 | tf_op jit(solution)/shard_map/reduce_scatter | solution.py:73
  390.4 0.0 copy-done.1
  390.4 2.7 add_convert_fusion
  (6 shorter events, 0.0 us)
Async XLA Ops:
  6.5 42.3 %copy-start.6 = (f32[3,512]{1,0:T(4,128)S(1)}, f32[3,512]{1,0:T(4,128)}, u32[]{:S(2)}) copy-start(f32[3,512]{1,0:T(4,128)} %param.16) | copy-start | bytes 18436
  6.5 66.2 %all-gather.10.cloned.1.call-start = ((), (), s32[]{:S(2)}) async-start(), calls=%async_computation.3 | async-start | bytes 2621440 | tf_op jit(solution)/shard_map/all_gather | solution.py:41
  7.3 89.6 %all-gather.12.cloned.1.call-start = ((), (), s32[]{:S(2)}) async-start(), calls=%async_computation.4 | async-start | bytes 2621440 | tf_op jit(solution)/shard_map/all_gather | solution.py:42
  8.0 58.2 %copy-start.2 = (bf16[512,512]{1,0:T(8,128)(2,1)S(1)}, bf16[512,512]{1,0:T(8,128)(2,1)}, u32[]{:S(2)}) copy-start(bf16[512,512]{1,0:T(8,128)(2,1)} %param.17) | copy-start | bytes 1572868
  8.0 125.9 %all-gather.8.cloned.1.call-start = ((), (), s32[]{:S(2)}) async-start(), calls=%async_computation.2 | async-start | bytes 2621440 | tf_op jit(solution)/shard_map/all_gather | solution.py:40
  8.1 18.3 %collective-permute-start = (bf16[512,512]{1,0:T(8,128)(2,1)}, bf16[512,512]{1,0:T(8,128)(2,1)S(1)}, u32[]{:S(2)}, u32[]{:S(2)}) collective-permute-start(bf16[512,512]{1,0:T(8,128)(2,1)} %param.17), channel_id=1, source_target_pairs={{0,2},{2,4},{4,6},{6,0},{1,3},{3,5},{5,7},{7,1},{8,10},{10,12},{12... | collective-permute-start | bytes 1572872 | tf_op jit(solution)/shard_map/ppermute | solution.py:50
  26.4 17.9 %collective-permute-start.1 = (bf16[512,512]{1,0:T(8,128)(2,1)S(1)}, bf16[512,512]{1,0:T(8,128)(2,1)S(1)}, u32[]{:S(2)}, u32[]{:S(2)}) collective-permute-start(bf16[512,512]{1,0:T(8,128)(2,1)S(1)} %collective-permute-done), channel_id=1, source_target_pairs={{0,2},{2,4},{4,6},{6,0},{1,3},{3,5},{5,7},{7,1},{8,10},{10,12},{12... | collective-permute-start | bytes 1572872 | tf_op jit(solution)/shard_map/ppermute | solution.py:50
  28.8 121.0 %reduce-scatter.3.cloned.1.call-start = ((), (), s32[]{:S(2)}) async-start(), calls=%async_computation.5 | async-start | bytes 3145728 | tf_op jit(solution)/shard_map/reduce_scatter | solution.py:55
  44.3 21.1 %copy-start.3 = (bf16[512,512]{1,0:T(8,128)(2,1)}, bf16[512,512]{1,0:T(8,128)(2,1)S(1)}, u32[]{:S(2)}) copy-start(bf16[512,512]{1,0:T(8,128)(2,1)S(1)} %collective-permute-done.1) | copy-start | bytes 1572868
  44.3 19.2 %collective-permute-start.2 = (bf16[512,512]{1,0:T(8,128)(2,1)S(1)}, bf16[512,512]{1,0:T(8,128)(2,1)S(1)}, u32[]{:S(2)}, u32[]{:S(2)}) collective-permute-start(bf16[512,512]{1,0:T(8,128)(2,1)S(1)} %collective-permute-done.1), channel_id=1, source_target_pairs={{0,2},{2,4},{4,6},{6,0},{1,3},{3,5},{5,7},{7,1},{8,10},{10,12},{12... | collective-permute-start | bytes 1572872 | tf_op jit(solution)/shard_map/ppermute | solution.py:50
  63.5 1.8 copy-start.4
  66.2 6.5 %copy-start = (bf16[512,2048]{1,0:T(8,128)(2,1)S(1)}, bf16[512,2048]{1,0:T(8,128)(2,1)}, u32[]{:S(2)}) copy-start(bf16[512,2048]{1,0:T(8,128)(2,1)} %param.11) | copy-start | bytes 6291460
  66.2 6.5 %copy-start.7 = (f32[2048]{0:T(1024)S(1)}, f32[2048]{0:T(1024)}, u32[]{:S(2)}) copy-start(f32[2048]{0:T(1024)} %param.12) | copy-start | bytes 24580
  139.9 11.6 %copy-start.5 = (f32[2048]{0:T(1024)S(1)}, f32[2048]{0:T(1024)}, u32[]{:S(2)}) copy-start(f32[2048]{0:T(1024)} %param.18) | copy-start | bytes 24580
  139.9 78.6 %all-gather.16.cloned.1.call-start = ((), (), s32[]{:S(2)}) async-start(), calls=%async_computation.7 | async-start | bytes 7208960 | tf_op jit(solution)/shard_map/all_gather | solution.py:65
  140.5 90.0 %all-gather.14.cloned.1.call-start = ((), (), s32[]{:S(2)}) async-start(), calls=%async_computation.6 | async-start | bytes 3145728 | tf_op jit(solution)/shard_map/all_gather | solution.py:68
  154.1 145.1 %all-gather.18.cloned.1.call-start = ((), (), s32[]{:S(2)}) async-start(), calls=%async_computation.8 | async-start | bytes 7208960 | tf_op jit(solution)/shard_map/all_gather | solution.py:66
  154.9 211.7 %all-gather.20.cloned.1.call-start = ((), (), s32[]{:S(2)}) async-start(), calls=%async_computation.9 | async-start | bytes 7208960 | tf_op jit(solution)/shard_map/all_gather | solution.py:72
  155.6 234.7 %reduce-scatter.5.cloned.1.call-start = ((), (), s32[]{:S(2)}) async-start(), calls=%async_computation.10 | async-start | bytes 3145728 | tf_op jit(solution)/shard_map/reduce_scatter | solution.py:73
  238.8 151.6 %copy-start.1 = (bf16[256,2048]{1,0:T(8,128)(2,1)S(1)}, bf16[256,2048]{1,0:T(8,128)(2,1)}, u32[]{:S(2)}) copy-start(bf16[256,2048]{1,0:T(8,128)(2,1)} %reduce-scatter.3.cloned.1.call-done) | copy-start | bytes 3145732
Sparse Core Ops, SparseCore 0:
  9.2 50.4 all-gather.9
  61.6 35.2 all-gather.11
  98.7 35.1 all-gather.7
  140.0 9.7 reduce-scatter.2
  151.5 66.9 all-gather.15
  219.9 10.5 all-gather.13
  232.4 66.8 all-gather.17
  301.1 65.5 all-gather.19
  380.6 9.7 reduce-scatter.4
